TPU v7x, 32 devices: a whole 2x2x4 slice. The times are simulated.
32 devices in a mesh: sp: 8 (over z, x), tp: 4 (over y, core).
Axes of the slice: x: 2, y: 2, z: 4, core: 2. Of those that a mesh axis runs over, the one named last changes fastest.
Arguments:
- tokens: bfloat16 [1024, 1024], P('sp', 'tp'), may hold values from -6 to 6
- norm_gain: float32 [3, 1024], replicated, may hold values from 0.1 to 1.9
- w_query: bfloat16 [3, 1024, 1024], P(None, 'sp', 'tp'), may hold values from -0.1875 to 0.1875
- w_key: bfloat16 [3, 1024, 1024], P(None, 'sp', 'tp'), may hold values from -0.1875 to 0.1875
- w_value: bfloat16 [3, 1024, 1024], P(None, 'sp', 'tp'), may hold values from -0.1875 to 0.1875
- w_out: bfloat16 [3, 1024, 1024], P(None, 'tp', 'sp'), may hold values from -0.5625 to 0.5625
- offset_bias: float32 [3, 16, 8, 16], P(None, 'tp'), may hold values from -3 to 3
- documents: int32 [1024], P('sp'), may hold values from 0 to 7, never falling along the last dimension, each value on 1 to 256 neighbouring positions
Outputs:
- mixed: bfloat16 [1024, 1024], P('sp', 'tp')
Inputs may be any that keep to these rules, and one draw needn't show every extreme that they name: `documents`: document numbers never fall along the token order, start at 0, and each document has 1 to 256 tokens.
All inputs are finite; a program needn't handle non-finite values.
Results may differ from a plain program's by a relative error of at most 0.02.
Values may be sent and summed in bfloat16 or wider, within the bound.
A program may use at most 64 MiB of HBM per device.

v0:
```python
import jax
import jax.numpy as jnp
from jax import lax
from jax.sharding import PartitionSpec as P

HEAD_DIM = 64
WIN_ROWS = 8
WIN_COLS = 16
LAYERS = 3
GRID_W = 32


EPS = 1e-06


def with_halo(shard, sides, width, wrap):
    for axis, dim in sides:
        count, length = lax.axis_size(axis), shard.shape[dim]
        up = [(i, (i + 1) % count) for i in range(count if wrap else count - 1)]
        down = [(j, i) for i, j in up]
        last = lax.slice_in_dim(shard, length - width, length, axis=dim)
        leading = lax.slice_in_dim(shard, 0, width, axis=dim)
        before = lax.ppermute(last, axis, up)
        after = lax.ppermute(leading, axis, down)
        shard = jnp.concatenate([before, shard, after], axis=dim)
    return shard


def rms_rows(stream, gain_row):
    values = stream.astype(jnp.float32)
    mean_sq = jnp.mean(values * values, axis=-1, keepdims=True)
    return (values * lax.rsqrt(mean_sq + EPS) * gain_row).astype(jnp.bfloat16)


def head_norm(heads_raw):
    values = heads_raw.astype(jnp.float32)
    mean_sq = jnp.mean(values * values, axis=-1, keepdims=True)
    return (values * lax.rsqrt(mean_sq + EPS)).astype(jnp.bfloat16)


def attend(queries, fringe, seg_own, seg_fringe, bias_layer):
    row_count, grid_width, head_count, head_width = queries.shape
    key_rows = jnp.stack(
        [fringe[row_lag : row_lag + row_count] for row_lag in range(WIN_ROWS)], axis=1
    )
    seg_rows = jnp.stack(
        [seg_fringe[row_lag : row_lag + row_count] for row_lag in range(WIN_ROWS)], axis=1
    )
    key_part = key_rows[..., :head_width]
    value_part = key_rows[..., head_width:]
    scores = jnp.einsum(
        "rchd,rjkhd->rhcjk", queries, key_part, preferred_element_type=jnp.float32
    ) * head_width ** (-0.5)
    column = jnp.arange(grid_width)
    col_offset = column[None, :] - column[:, None] + WIN_COLS // 2
    inside = (col_offset >= 0) & (col_offset < WIN_COLS)
    bias_table = bias_layer[:, :, jnp.clip(col_offset, 0, WIN_COLS - 1)]
    scores = scores + jnp.transpose(bias_table, (0, 2, 1, 3))[None]
    same_doc = seg_rows[:, None, None, :, :] == seg_own[:, None, :, None, None]
    allowed = same_doc & inside[None, None, :, None, :]
    scores = jnp.where(allowed, scores, -1e30)
    flat = scores.reshape(row_count, head_count, grid_width, WIN_ROWS * grid_width)
    attn_probs = jax.nn.softmax(flat, axis=-1).astype(jnp.bfloat16)
    attn_probs = attn_probs.reshape(row_count, head_count, grid_width, WIN_ROWS, grid_width)
    mixed_heads = jnp.einsum(
        "rhcjk,rjkhd->rchd", attn_probs, value_part, preferred_element_type=jnp.float32
    )
    return mixed_heads.astype(jnp.bfloat16)


def body(tokens, norm_gain, w_query, w_key, w_value, w_out, offset_bias, documents):
    token_count = tokens.shape[0]
    row_count = token_count // GRID_W
    reach_rows = WIN_ROWS // 2
    head_count = offset_bias.shape[1]
    seg_own = (documents + 1).reshape(row_count, GRID_W)
    seg_fringe = with_halo(seg_own, (("sp", 0),), reach_rows, False)
    collected = (
        lax.all_gather(w_query, "sp", axis=1, tiled=True),
        lax.all_gather(w_key, "sp", axis=1, tiled=True),
        lax.all_gather(w_value, "sp", axis=1, tiled=True),
        lax.all_gather(w_out, "sp", axis=2, tiled=True),
    )
    stream = tokens
    for layer_index in range(LAYERS):
        gathered = lax.all_gather(stream, "tp", axis=1, tiled=True)
        normed = rms_rows(gathered, norm_gain[layer_index])
        query_raw = jnp.dot(normed, collected[0][layer_index], preferred_element_type=jnp.float32)
        key_raw = jnp.dot(normed, collected[1][layer_index], preferred_element_type=jnp.float32)
        value_raw = jnp.dot(normed, collected[2][layer_index], preferred_element_type=jnp.float32)
        query_heads = head_norm(
            query_raw.astype(jnp.bfloat16).reshape(row_count, GRID_W, head_count, HEAD_DIM)
        )
        key_heads = head_norm(
            key_raw.astype(jnp.bfloat16).reshape(row_count, GRID_W, head_count, HEAD_DIM)
        )
        value_heads = value_raw.astype(jnp.bfloat16).reshape(
            row_count, GRID_W, head_count, HEAD_DIM
        )
        key_value = jnp.concatenate([key_heads, value_heads], axis=-1)
        fringe = with_halo(key_value, (("sp", 0),), reach_rows, False)
        attended = attend(query_heads, fringe, seg_own, seg_fringe, offset_bias[layer_index])
        attended = attended.reshape(token_count, head_count * HEAD_DIM)
        partial_sums = jnp.dot(
            attended, collected[3][layer_index], preferred_element_type=jnp.float32
        )
        stream = (
            lax.psum_scatter(
                partial_sums.astype(jnp.bfloat16), "tp", scatter_dimension=1, tiled=True
            )
            .astype(jnp.float32)
            .astype(jnp.bfloat16)
        )
    return stream


def solution(mesh):
    return jax.shard_map(
        body,
        mesh=mesh,
        in_specs=(
            P("sp", "tp"),
            P(),
            P(None, "sp", "tp"),
            P(None, "sp", "tp"),
            P(None, "sp", "tp"),
            P(None, "tp", "sp"),
            P(None, "tp", None, None),
            P("sp"),
        ),
        out_specs=P("sp", "tp"),
        check_vma=False,
    )
```

profile of v0, /device:TPU:9, one launch (start us, length us, event | category | flops | bytes accessed | tf_op | source)
XLA Modules:
  0.0 309.6 jit_solution(167499018848324964)
XLA Ops:
  6.5 0.7 all-gather.5.cloned.1.call-update
  7.3 0.7 all-gather.7.cloned.1.call-update
  8.1 0.7 all-gather.9.cloned.1.call-update
  9.5 3.1 %collective-permute-start.2 = (s32[4,32]{1,0:T(4,128)S(1)}, s32[4,32]{1,0:T(4,128)S(1)}, u32[]{:S(2)}, u32[]{:S(2)}) collective-permute-start(s32[4,32]{1,0:T(4,128)S(1)} %reshape.186), channel_id=1, source_target_pairs={{0,4},{4,8},{8,12},{12,16},{16,20},{20,24},{24,28},{1,5},{5,9},{9,... | collective-permute-start | bytes 1544 | tf_op jit(solution)/shard_map/ppermute | solution.py:23
  12.6 3.1 collective-permute-start.3
  15.8 7.1 %all_gather.21 = bf16[128,1024]{1,0:T(8,128)(2,1)S(1)} all-gather(bf16[128,256]{1,0:T(8,128)(2,1)} %param.8), channel_id=1, replica_groups=mesh['sp'=8,'tp'=4] {'tp'}, dimensions={1}, use_global_device_ids=true | all-gather | bytes 327680 | tf_op jit(solution)/shard_map/all_gather | solution.py:86
  23.0 0.8 fusion.79
  23.9 0.8 fusion.78
  24.9 3.5 %gather_fusion = f32[1024,4,8]{2,1,0:T(4,128)S(1)} fusion(f32[4,8,16]{1,0,2:T(4,128)S(1)} %bitcast.251, s32[1024]{0:T(1024)S(1)} %broadcast_clamp_fusion), kind=kCustom, calls=%fused_computation | custom fusion | bytes 266240 | tf_op jit(solution)/shard_map/gather | solution.py:57
  28.4 1.3 copy.150
  30.0 23.7 %all-gather.5.cloned.1.call-done = bf16[3,1024,256]{2,1,0:T(8,128)(2,1)} async-done(((bf16[3,128,256]{2,1,0:T(8,128)(2,1)}), bf16[3,1024,256]{2,1,0:T(8,128)(2,1)}) %all-gather.5.cloned.1.call-update) | async-done | bytes 1572880 | tf_op jit(solution)/shard_map/all_gather | solution.py:80
  53.8 1.3 fusion.17
  55.7 43.0 %all-gather.7.cloned.1.call-done = bf16[3,1024,256]{2,1,0:T(8,128)(2,1)} async-done(((bf16[3,128,256]{2,1,0:T(8,128)(2,1)}), bf16[3,1024,256]{2,1,0:T(8,128)(2,1)}) %all-gather.7.cloned.1.call-update) | async-done | bytes 1572880 | tf_op jit(solution)/shard_map/all_gather | solution.py:81
  98.8 1.3 convolution_convert_fusion.10
  100.4 2.2 collective-permute-start
  102.6 4.0 %collective-permute-start.1 = (bf16[4,32,4,128]{3,1,2,0:T(8,128)(2,1)S(1)}, bf16[4,32,4,128]{3,1,2,0:T(8,128)(2,1)S(1)}, u32[]{:S(2)}, u32[]{:S(2)}) collective-permute-start(bf16[4,32,4,128]{3,1,2,0:T(8,128)(2,1)S(1)} %pad_maximum_fusion.3), channel_id=1, source_target_pairs={{4,0},{8,4},{12,8},{16,12},{20,16},{24,20},{28,24},{5,1},{9,5},{13... | collective-permute-start | bytes 393224 | tf_op jit(solution)/shard_map/ppermute | solution.py:24
  106.6 37.5 %all-gather.9.cloned.1.call-done = bf16[3,1024,256]{2,1,0:T(8,128)(2,1)} async-done(((bf16[3,128,256]{2,1,0:T(8,128)(2,1)}), bf16[3,1024,256]{2,1,0:T(8,128)(2,1)}) %all-gather.9.cloned.1.call-update) | async-done | bytes 1572880 | tf_op jit(solution)/shard_map/all_gather | solution.py:79
  144.1 1.3 fusion.16
  146.4 0.7 fusion.3
  147.7 1.1 fusion.11
  149.0 40.2 %all-gather.11.cloned.1.call-done = bf16[3,256,1024]{2,1,0:T(8,128)(2,1)} async-done(((bf16[3,256,128]{2,1,0:T(8,128)(2,1)}), bf16[3,256,1024]{2,1,0:T(8,128)(2,1)}) %all-gather.11.cloned.1.call-update) | async-done | bytes 1572880 | tf_op jit(solution)/shard_map/all_gather | solution.py:82
  189.2 2.0 convolution_convert_fusion.2
  191.3 3.6 %gather_fusion.1 = f32[1024,4,8]{2,1,0:T(4,128)S(1)} fusion(f32[4,8,16]{1,0,2:T(4,128)S(1)} %bitcast.252, s32[1024]{0:T(1024)S(1)} %broadcast_clamp_fusion), kind=kCustom, calls=%fused_computation.1 | custom fusion | bytes 266240 | tf_op jit(solution)/shard_map/gather | solution.py:57
  194.9 1.3 copy.167
  196.1 15.0 %reduce-scatter.4.cloned.1.call-done = bf16[128,256]{1,0:T(8,128)(2,1)} async-done(((bf16[128,1024]{1,0:T(8,128)(2,1)}), bf16[128,256]{1,0:T(8,128)(2,1)}) %reduce-scatter.4.cloned.1.call-update) | async-done | bytes 65552 | tf_op jit(solution)/shard_map/reduce_scatter | solution.py:108
  211.1 6.8 %all_gather.26 = bf16[128,1024]{1,0:T(8,128)(2,1)S(1)} all-gather(bf16[128,256]{1,0:T(8,128)(2,1)} %reduce-scatter.4.cloned.1.call-done), channel_id=1, replica_groups=mesh['sp'=8,'tp'=4] {'tp'}, dimensions={1}, use_global_device_ids=true | all-gather | bytes 327680 | tf_op jit(solution)/shard_map/all_gather | solution.py:86
  218.1 1.3 fusion.15
  220.0 1.3 convolution_convert_fusion.7
  221.6 3.1 %collective-permute-start.4 = (bf16[4,32,4,128]{3,1,2,0:T(8,128)(2,1)S(1)}, bf16[4,32,4,128]{3,1,2,0:T(8,128)(2,1)S(1)}, u32[]{:S(2)}, u32[]{:S(2)}) collective-permute-start(bf16[4,32,4,128]{3,1,2,0:T(8,128)(2,1)S(1)} %pad_maximum_fusion.4), channel_id=1, source_target_pairs={{0,4},{4,8},{8,12},{12,16},{16,20},{20,24},{24,28},{1,5},{5,9},{9,... | collective-permute-start | bytes 393224 | tf_op jit(solution)/shard_map/ppermute | solution.py:23
  224.7 3.3 %collective-permute-start.5 = (bf16[4,32,4,128]{3,1,2,0:T(8,128)(2,1)S(1)}, bf16[4,32,4,128]{3,1,2,0:T(8,128)(2,1)S(1)}, u32[]{:S(2)}, u32[]{:S(2)}) collective-permute-start(bf16[4,32,4,128]{3,1,2,0:T(8,128)(2,1)S(1)} %pad_maximum_fusion.4), channel_id=1, source_target_pairs={{4,0},{8,4},{12,8},{16,12},{20,16},{24,20},{28,24},{5,1},{9,5},{13... | collective-permute-start | bytes 393224 | tf_op jit(solution)/shard_map/ppermute | solution.py:24
  228.0 1.3 fusion.14
  230.0 2.7 collective-permute-done.5
  233.0 0.7 fusion.4
  234.2 1.1 fusion.10
  235.5 2.0 convolution_convert_fusion.1
  237.7 3.5 %gather_fusion.2 = f32[1024,4,8]{2,1,0:T(4,128)S(1)} fusion(f32[4,8,16]{1,0,2:T(4,128)S(1)} %bitcast.250, s32[1024]{0:T(1024)S(1)} %broadcast_clamp_fusion), kind=kCustom, calls=%fused_computation.2 | custom fusion | bytes 266240 | tf_op jit(solution)/shard_map/gather | solution.py:57
  241.2 1.3 copy.184
  242.5 14.4 %reduce-scatter.6.cloned.1.call-done = bf16[128,256]{1,0:T(8,128)(2,1)} async-done(((bf16[128,1024]{1,0:T(8,128)(2,1)}), bf16[128,256]{1,0:T(8,128)(2,1)}) %reduce-scatter.6.cloned.1.call-update) | async-done | bytes 65552 | tf_op jit(solution)/shard_map/reduce_scatter | solution.py:108
  256.9 6.9 %all_gather.27 = bf16[128,1024]{1,0:T(8,128)(2,1)S(1)} all-gather(bf16[128,256]{1,0:T(8,128)(2,1)} %reduce-scatter.6.cloned.1.call-done), channel_id=1, replica_groups=mesh['sp'=8,'tp'=4] {'tp'}, dimensions={1}, use_global_device_ids=true | all-gather | bytes 327680 | tf_op jit(solution)/shard_map/all_gather | solution.py:86
  263.9 1.3 fusion.13
  265.9 1.3 convolution_convert_fusion.4
  267.5 3.1 collective-permute-start.6
  270.6 3.1 %collective-permute-start.7 = (bf16[4,32,4,128]{3,1,2,0:T(8,128)(2,1)S(1)}, bf16[4,32,4,128]{3,1,2,0:T(8,128)(2,1)S(1)}, u32[]{:S(2)}, u32[]{:S(2)}) collective-permute-start(bf16[4,32,4,128]{3,1,2,0:T(8,128)(2,1)S(1)} %pad_maximum_fusion.5), channel_id=1, source_target_pairs={{4,0},{8,4},{12,8},{16,12},{20,16},{24,20},{28,24},{5,1},{9,5},{13... | collective-permute-start | bytes 393224 | tf_op jit(solution)/shard_map/ppermute | solution.py:24
  273.7 1.3 fusion.12
  275.7 2.9 collective-permute-done.7
  280.1 1.1 fusion.9
  281.4 2.0 convolution_convert_fusion
  283.4 19.3 %reduce-scatter.8.cloned.1.call-done = bf16[128,256]{1,0:T(8,128)(2,1)} async-done(((bf16[128,1024]{1,0:T(8,128)(2,1)}), bf16[128,256]{1,0:T(8,128)(2,1)}) %reduce-scatter.8.cloned.1.call-update) | async-done | bytes 65552 | tf_op jit(solution)/shard_map/reduce_scatter | solution.py:108
  (117 shorter events, 10.6 us)
Async XLA Ops:
  6.5 47.3 %all-gather.5.cloned.1.call-start = ((), (), s32[]{:S(2)}) async-start(), calls=%async_computation.3 | async-start | bytes 1769472 | tf_op jit(solution)/shard_map/all_gather | solution.py:80
  7.3 91.5 %all-gather.7.cloned.1.call-start = ((), (), s32[]{:S(2)}) async-start(), calls=%async_computation.4 | async-start | bytes 1769472 | tf_op jit(solution)/shard_map/all_gather | solution.py:81
  8.0 136.1 %all-gather.9.cloned.1.call-start = ((), (), s32[]{:S(2)}) async-start(), calls=%async_computation.5 | async-start | bytes 1769472 | tf_op jit(solution)/shard_map/all_gather | solution.py:79
  8.7 180.4 %all-gather.11.cloned.1.call-start = ((), (), s32[]{:S(2)}) async-start(), calls=%async_computation.6 | async-start | bytes 1769472 | tf_op jit(solution)/shard_map/all_gather | solution.py:82
  9.5 20.2 %collective-permute-start.2 = (s32[4,32]{1,0:T(4,128)S(1)}, s32[4,32]{1,0:T(4,128)S(1)}, u32[]{:S(2)}, u32[]{:S(2)}) collective-permute-start(s32[4,32]{1,0:T(4,128)S(1)} %reshape.186), channel_id=1, source_target_pairs={{0,4},{4,8},{8,12},{12,16},{16,20},{20,24},{24,28},{1,5},{5,9},{9,... | collective-permute-start | bytes 1544 | tf_op jit(solution)/shard_map/ppermute | solution.py:23
  12.6 17.1 %collective-permute-start.3 = (s32[4,32]{1,0:T(4,128)S(1)}, s32[4,32]{1,0:T(4,128)S(1)}, u32[]{:S(2)}, u32[]{:S(2)}) collective-permute-start(s32[4,32]{1,0:T(4,128)S(1)} %reshape.186), channel_id=1, source_target_pairs={{4,0},{8,4},{12,8},{16,12},{20,16},{24,20},{28,24},{5,1},{9,5},{13... | collective-permute-start | bytes 1544 | tf_op jit(solution)/shard_map/ppermute | solution.py:24
  15.7 195.4 %reduce-scatter.4.cloned.1.call-start = ((), (), s32[]{:S(2)}) async-start(), calls=%async_computation.7 | async-start | bytes 327680 | tf_op jit(solution)/shard_map/reduce_scatter | solution.py:108
  100.4 45.7 %collective-permute-start = (bf16[4,32,4,128]{3,1,2,0:T(8,128)(2,1)S(1)}, bf16[4,32,4,128]{3,1,2,0:T(8,128)(2,1)S(1)}, u32[]{:S(2)}, u32[]{:S(2)}) collective-permute-start(bf16[4,32,4,128]{3,1,2,0:T(8,128)(2,1)S(1)} %pad_maximum_fusion.3), channel_id=1, source_target_pairs={{0,4},{4,8},{8,12},{12,16},{16,20},{20,24},{24,28},{1,5},{5,9},{9,... | collective-permute-start | bytes 393224 | tf_op jit(solution)/shard_map/ppermute | solution.py:23
  102.6 43.5 %collective-permute-start.1 = (bf16[4,32,4,128]{3,1,2,0:T(8,128)(2,1)S(1)}, bf16[4,32,4,128]{3,1,2,0:T(8,128)(2,1)S(1)}, u32[]{:S(2)}, u32[]{:S(2)}) collective-permute-start(bf16[4,32,4,128]{3,1,2,0:T(8,128)(2,1)S(1)} %pad_maximum_fusion.3), channel_id=1, source_target_pairs={{4,0},{8,4},{12,8},{16,12},{20,16},{24,20},{28,24},{5,1},{9,5},{13... | collective-permute-start | bytes 393224 | tf_op jit(solution)/shard_map/ppermute | solution.py:24
  191.2 65.8 %reduce-scatter.6.cloned.1.call-start = ((), (), s32[]{:S(2)}) async-start(), calls=%async_computation.8 | async-start | bytes 327680 | tf_op jit(solution)/shard_map/reduce_scatter | solution.py:108
  221.6 8.3 %collective-permute-start.4 = (bf16[4,32,4,128]{3,1,2,0:T(8,128)(2,1)S(1)}, bf16[4,32,4,128]{3,1,2,0:T(8,128)(2,1)S(1)}, u32[]{:S(2)}, u32[]{:S(2)}) collective-permute-start(bf16[4,32,4,128]{3,1,2,0:T(8,128)(2,1)S(1)} %pad_maximum_fusion.4), channel_id=1, source_target_pairs={{0,4},{4,8},{8,12},{12,16},{16,20},{20,24},{24,28},{1,5},{5,9},{9,... | collective-permute-start | bytes 393224 | tf_op jit(solution)/shard_map/ppermute | solution.py:23
  224.7 7.9 %collective-permute-start.5 = (bf16[4,32,4,128]{3,1,2,0:T(8,128)(2,1)S(1)}, bf16[4,32,4,128]{3,1,2,0:T(8,128)(2,1)S(1)}, u32[]{:S(2)}, u32[]{:S(2)}) collective-permute-start(bf16[4,32,4,128]{3,1,2,0:T(8,128)(2,1)S(1)} %pad_maximum_fusion.4), channel_id=1, source_target_pairs={{4,0},{8,4},{12,8},{16,12},{20,16},{24,20},{28,24},{5,1},{9,5},{13... | collective-permute-start | bytes 393224 | tf_op jit(solution)/shard_map/ppermute | solution.py:24
  237.6 65.2 %reduce-scatter.8.cloned.1.call-start = ((), (), s32[]{:S(2)}) async-start(), calls=%async_computation.9 | async-start | bytes 327680 | tf_op jit(solution)/shard_map/reduce_scatter | solution.py:108
  267.5 8.1 %collective-permute-start.6 = (bf16[4,32,4,128]{3,1,2,0:T(8,128)(2,1)S(1)}, bf16[4,32,4,128]{3,1,2,0:T(8,128)(2,1)S(1)}, u32[]{:S(2)}, u32[]{:S(2)}) collective-permute-start(bf16[4,32,4,128]{3,1,2,0:T(8,128)(2,1)S(1)} %pad_maximum_fusion.5), channel_id=1, source_target_pairs={{0,4},{4,8},{8,12},{12,16},{16,20},{20,24},{24,28},{1,5},{5,9},{9,... | collective-permute-start | bytes 393224 | tf_op jit(solution)/shard_map/ppermute | solution.py:23
  270.6 7.9 %collective-permute-start.7 = (bf16[4,32,4,128]{3,1,2,0:T(8,128)(2,1)S(1)}, bf16[4,32,4,128]{3,1,2,0:T(8,128)(2,1)S(1)}, u32[]{:S(2)}, u32[]{:S(2)}) collective-permute-start(bf16[4,32,4,128]{3,1,2,0:T(8,128)(2,1)S(1)} %pad_maximum_fusion.5), channel_id=1, source_target_pairs={{4,0},{8,4},{12,8},{16,12},{20,16},{24,20},{28,24},{5,1},{9,5},{13... | collective-permute-start | bytes 393224 | tf_op jit(solution)/shard_map/ppermute | solution.py:24
Sparse Core Ops, SparseCore 0:
  9.5 44.2 all-gather.4
  56.0 42.7 all-gather.6
  101.0 43.0 all-gather.8
  146.0 43.1 all-gather.10
  191.5 19.6 reduce-scatter.3
  237.7 19.2 reduce-scatter.5
  283.6 19.1 reduce-scatter.7
where the time goes:
time: 313 us; the launch traced here: 310 us
  waiting for transfers between devices  201 us (64%)
  starting transfers between devices  25.1 us (8%)
  matrix products  23 us (7%)
  blocking collectives  20.8 us (7%)
  local copies, waits for them, and re-layouts  19.3 us (6%)
  between operations  14.2 us (5%)
  other arithmetic  6.3 us (2%)
    reduce_scatter x3, waiting for transfers between devices, body(): lax.psum_scatter(partial_sums.astype(jnp.bfloat16), 'tp', scatter_dimensi...  48.7 us
    all_gather x1, waiting for transfers between devices, body(): lax.all_gather(w_value, 'sp', axis=1, tiled=True)  43 us
    all_gather x1, waiting for transfers between devices, body(): lax.all_gather(w_out, 'sp', axis=2, tiled=True)  40.2 us
    all_gather x1, waiting for transfers between devices, body(): lax.all_gather(w_query, 'sp', axis=1, tiled=True)  37.5 us
    all_gather x1, waiting for transfers between devices, body(): lax.all_gather(w_key, 'sp', axis=1, tiled=True)  23.7 us
    all_gather x3, blocking collectives, body(): gathered = lax.all_gather(stream, 'tp', axis=1, tiled=True)  20.8 us
    gather x6, local copies, waits for them, and re-layouts, attend(): bias_table = bias_layer[:, :, jnp.clip(col_offset, 0, WIN_COLS - 1)]  14.4 us
    ppermute x4, starting transfers between devices, with_halo(): after = lax.ppermute(leading, axis, down)  13.4 us
  transfers between devices with their start and end apart: 15, of which 9 were waited for; matrix products, arithmetic and copies ran while one was open for 10% of the time, Pallas kernels for 0%

commit v1 on v0

v1 whole, which is shorter than its diff:
```python
import functools

import jax
import jax.numpy as jnp
from jax import lax
from jax.experimental import pallas as pl
from jax.experimental.pallas import tpu as pltpu
from jax.sharding import PartitionSpec as P

HEAD_DIM = 64
WIN_ROWS = 8
WIN_COLS = 16
GRID_W = 32
EPS = 1e-06
MESH = pl.DeviceIdType.MESH
F32, BF16 = jnp.float32, jnp.bfloat16
K, V, Q, O = 0, 1, 2, 3


def kernel(n, nt, xs, layers, heads, tok_ref, gain_ref, wq_ref, wk_ref, wv_ref, wo_ref, bias_ref, doc_ref,
           out_ref, wbuf, obuf, xg, kv, part, s1, cs, s2, att, strip, dmask, docs,
           own_sem, w_send, w_recv, g_send, g_recv, h_send, h_recv, d_send, d_recv,
           r_send, r_recv, y_send, y_recv, b_send, b_recv):
    me, tp = lax.axis_index("sp"), lax.axis_index("tp")
    zs = n // xs
    toks, feat = tok_ref.shape
    reach = (WIN_ROWS // 2) * GRID_W
    after = reach - GRID_W
    wrows = wq_ref.shape[1]

    def pos_of(sp):
        z, x = sp // xs, sp % xs
        odd = x % 2
        return x * zs + z * (1 - odd) + (zs - 1 - z) * odd

    def sp_of(pos):
        x, z = pos // zs, pos % zs
        odd = x % 2
        return (z * (1 - odd) + (zs - 1 - z) * odd) * xs + x

    pos = pos_of(me)
    right, left = sp_of((pos + 1) % n), sp_of((pos + n - 1) % n)
    core = tp % 2
    mate = tp + 1 - 2 * core
    ymate = (tp + nt // 2) % nt
    has_prev = (me + n - 1) // n
    has_next = 1 - (me + 1) // n

    owns = []
    for l in range(layers):
        for c, ref in ((K, wk_ref), (V, wv_ref), (Q, wq_ref), (O, wo_ref)):
            dst = obuf.at[l, me] if c == O else wbuf.at[l, c, pl.ds(me * wrows, wrows)]
            copy = pltpu.make_async_copy(ref.at[l], dst, own_sem.at[l, c])
            copy.start()
            owns.append(copy)

    barrier = pltpu.get_barrier_semaphore()
    for peer in (left, right):
        pl.semaphore_signal(barrier, inc=1, device_id=(peer, tp), device_id_type=MESH)
    for d in range(1, nt):
        pl.semaphore_signal(barrier, inc=1, device_id=(me, (tp + d) % nt), device_id_type=MESH)

    @pl.when(me > 0)
    def _():
        pl.semaphore_signal(barrier, inc=1, device_id=(me - 1, tp), device_id_type=MESH)

    @pl.when(me < n - 1)
    def _():
        pl.semaphore_signal(barrier, inc=1, device_id=(me + 1, tp), device_id_type=MESH)

    pl.semaphore_wait(barrier, 1 + nt + has_prev + has_next)

    pending = []

    def remote(src, dst, send, recv, device):
        return pltpu.make_async_remote_copy(src_ref=src, dst_ref=dst, send_sem=send, recv_sem=recv,
                                            device_id=device, device_id_type=MESH)

    half = n // 2
    RIGHTLAST, LEFTLAST = (K, V), (Q, O)

    def w_chunks(direction, step):
        if step < half:
            return (K, V, Q, O)
        if step == half:
            return RIGHTLAST if direction == 0 else LEFTLAST
        return ()

    def w_copy(direction, l, step, c):
        if direction == 0:
            origin, peer = sp_of((pos + n - (step - 1)) % n), right
        else:
            origin, peer = sp_of((pos + step - 1) % n), left
        ref = obuf.at[l, origin] if c == O else wbuf.at[l, c, pl.ds(origin * wrows, wrows)]
        return remote(ref, ref, w_send.at[direction, l, step - 1, c], w_recv.at[direction, l, step - 1, c],
                      (peer, tp))

    def w_arrive(direction, l, step, c):
        if direction == 0:
            origin = sp_of((pos + n - step) % n)
        else:
            origin = sp_of((pos + step) % n)
        ref = obuf.at[l, origin] if c == O else wbuf.at[l, c, pl.ds(origin * wrows, wrows)]
        remote(ref, ref, w_send.at[direction, l, step - 1, c], w_recv.at[direction, l, step - 1, c],
               (right if direction == 0 else left, tp)).wait_recv()

    def w_first(l):
        for c in range(4):
            owns[l * 4 + c].wait()
            for direction in range(2):
                if c in w_chunks(direction, 1):
                    copy = w_copy(direction, l, 1, c)
                    copy.start()
                    pending.append(copy)

    def w_step(l, step):
        for c in range(4):
            for direction in range(2):
                if c in w_chunks(direction, step):
                    w_arrive(direction, l, step, c)
                if c in w_chunks(direction, step + 1):
                    copy = w_copy(direction, l, step + 1, c)
                    copy.start()
                    pending.append(copy)

    tasks = []
    for l in range(layers):
        if l:
            tasks.append((l, functools.partial(w_first, l)))
        for step in range(1, half + 1):
            tasks.append((l, functools.partial(w_step, l, step)))

    def work(count, limit):
        while count > 0 and tasks and tasks[0][0] <= limit:
            tasks.pop(0)[1]()
            count -= 1

    w_first(0)
    gathers = []
    for d in range(1, nt):
        copy = remote(tok_ref, xg.at[0, tp], g_send.at[d - 1], g_recv.at[d - 1], (me, (tp + d) % nt))
        copy.start()
        gathers.append(copy)
    xg[0, tp] = tok_ref[...]

    def to_prev(src, dst, k):
        return remote(src, dst, h_send.at[0, k], h_recv.at[0, k], (jnp.maximum(me - 1, 0), tp))

    def to_next(src, dst, k):
        return remote(src, dst, h_send.at[1, k], h_recv.at[1, k], (jnp.minimum(me + 1, n - 1), tp))

    doc_prev = remote(doc_ref, docs.at[2], d_send.at[0], d_recv.at[0], ((me + n - 1) % n, tp))
    doc_next = remote(doc_ref, docs.at[0], d_send.at[1], d_recv.at[1], ((me + 1) % n, tp))

    @pl.when(me > 0)
    def _():
        doc_prev.start()

    @pl.when(me < n - 1)
    def _():
        doc_next.start()

    docs[1] = doc_ref[...]

    @pl.when(me == 0)
    def _():
        docs[0] = jnp.full_like(doc_ref, -1)
        for l in range(layers):
            kv[l, 0:reach] = jnp.zeros((reach, 2 * feat), BF16)

    @pl.when(me == n - 1)
    def _():
        docs[2] = jnp.full_like(doc_ref, -1)
        for l in range(layers):
            kv[l, reach + toks:reach + toks + after] = jnp.zeros((after, 2 * feat), BF16)

    for l in range(layers):
        for h in range(heads):
            row = jnp.broadcast_to(bias_ref[l * heads + h:l * heads + h + 1, :], (GRID_W, WIN_ROWS * GRID_W))
            strip[l, h] = pltpu.roll(row, WIN_ROWS * GRID_W - WIN_COLS // 2, 1, stride=1, stride_axis=0)

    work(1, 0)

    @pl.when(me > 0)
    def _():
        doc_next.wait_recv()

    @pl.when(me < n - 1)
    def _():
        doc_prev.wait_recv()

    seg = [docs[i].astype(F32) for i in range(3)]
    seg_row = jnp.concatenate(seg, axis=1)
    seg_col = jnp.transpose(jnp.broadcast_to(seg[1], (toks, toks)))
    lane = lax.broadcasted_iota(jnp.int32, (GRID_W, WIN_ROWS * GRID_W), 1) % GRID_W
    col = lax.broadcasted_iota(jnp.int32, (GRID_W, WIN_ROWS * GRID_W), 0)
    off = lane - col + WIN_COLS // 2
    inside = (off >= 0) & (off < WIN_COLS)
    rows = toks // GRID_W
    for r in range(rows):
        keys = seg_row[:, r * GRID_W:(r + WIN_ROWS) * GRID_W]
        mine = seg_col[r * GRID_W:(r + 1) * GRID_W, 0:1]
        dmask[r] = jnp.where(inside & (keys == mine), 0.0, -1e30)

    work(1, 0)
    for copy in gathers:
        copy.wait_recv()

    def head_norm(raw, scale):
        raw = raw.astype(BF16).astype(F32)
        sq = raw * raw
        outs = []
        for h in range(heads):
            cut = slice(h * HEAD_DIM, (h + 1) * HEAD_DIM)
            mean = jnp.sum(sq[:, cut], axis=-1, keepdims=True) * (1.0 / HEAD_DIM)
            outs.append(raw[:, cut] * (lax.rsqrt(mean + EPS) * scale))
        return jnp.concatenate(outs, axis=1).astype(BF16)

    for l in range(layers):
        x = [xg[l, q].astype(F32) for q in range(nt)]
        total = sum(jnp.sum(v * v, axis=-1, keepdims=True) for v in x)
        inv = lax.rsqrt(total * (1.0 / (nt * feat)) + EPS)
        normed = jnp.concatenate(
            [(x[q] * inv * gain_ref[l:l + 1, q * feat:(q + 1) * feat]).astype(BF16) for q in range(nt)], axis=1)
        while tasks and tasks[0][0] <= l:
            work(1, l)
        if l + 1 < layers:
            work(1, l + 1)

        own = slice(reach, reach + toks)
        kv[l, own, 0:feat] = head_norm(jnp.dot(normed, wbuf[l, K], preferred_element_type=F32), 1.0)
        kv[l, own, feat:2 * feat] = jnp.dot(normed, wbuf[l, V], preferred_element_type=F32).astype(BF16)
        up = to_next(kv.at[l, own], kv.at[l, 0:reach], l)
        down = to_prev(kv.at[l, reach:reach + after], kv.at[l, reach + toks:reach + toks + after], l)

        @pl.when(me < n - 1)
        def _():
            up.start()

        @pl.when(me > 0)
        def _():
            down.start()

        query = head_norm(jnp.dot(normed, wbuf[l, Q], preferred_element_type=F32), HEAD_DIM ** -0.5)
        work(1, l + 1)

        @pl.when(me > 0)
        def _():
            up.wait_recv()

        @pl.when(me < n - 1)
        def _():
            down.wait_recv()

        for h in range(heads):
            cut = slice(h * HEAD_DIM, (h + 1) * HEAD_DIM)
            for r in range(rows):
                win = slice(r * GRID_W, (r + WIN_ROWS) * GRID_W)
                qr = query[r * GRID_W:(r + 1) * GRID_W, cut]
                s = lax.dot_general(qr, kv[l, win, cut], (((1,), (1,)), ((), ())), preferred_element_type=F32)
                p = jnp.exp(s + strip[l, h] + dmask[r])
                den = jnp.sum(p, axis=-1, keepdims=True)
                vals = kv[l, win, feat + h * HEAD_DIM:feat + (h + 1) * HEAD_DIM]
                o = jnp.dot(p.astype(BF16), vals, preferred_element_type=F32)
                att[r * GRID_W:(r + 1) * GRID_W, cut] = (o / den).astype(BF16)

        work(1, l + 1)
        a = att[...]
        per = feat // wo_ref.shape[2]

        def mix(q):
            return jnp.concatenate(
                [jnp.dot(a, obuf[l, q * per + i], preferred_element_type=F32) for i in range(per)], axis=1)

        s1c = []
        for j in range(2):
            part[l, j] = mix(1 - core + 2 * j).astype(BF16)
            copy = remote(part.at[l, j], s1.at[l, j], r_send.at[l, j], r_recv.at[l, j], (me, mate))
            copy.start()
            s1c.append(copy)
            pending.append(copy)
        mine = [mix(core + 2 * j) for j in range(2)]
        last = l == layers - 1
        if not last:
            s2c = []
            for j in range(2):
                s1c[j].wait_recv()
                cs[l, j] = (mine[j] + s1[l, j].astype(F32)).astype(BF16)
                copy = remote(cs.at[l, j], s2.at[l, j], y_send.at[l, j], y_recv.at[l, j], (me, ymate))
                copy.start()
                s2c.append(copy)
                pending.append(copy)
            work(1, l + 1)
            s3c = []
            for j in range(2):
                s2c[j].wait_recv()
                slot = core + 2 * j
                xg[l + 1, slot] = (cs[l, j].astype(F32) + s2[l, j].astype(F32)).astype(BF16)
                copy = remote(xg.at[l + 1, slot], xg.at[l + 1, slot], b_send.at[l, j], b_recv.at[l, j], (me, mate))
                copy.start()
                s3c.append(copy)
                pending.append(copy)
            for j in range(2):
                s3c[j].wait_recv()
        else:
            y = tp // 2
            for j in range(2):
                s1c[j].wait_recv()
                cs[l, j] = (mine[j] + s1[l, j].astype(F32)).astype(BF16)
            copy = remote(cs.at[l, 1 - y], s2.at[l, 0], y_send.at[l, 0], y_recv.at[l, 0], (me, ymate))
            copy.start()
            pending.append(copy)
            copy.wait_recv()
            out_ref[...] = (cs[l, y].astype(F32) + s2[l, 0].astype(F32)).astype(BF16)

        @pl.when(me < n - 1)
        def _():
            up.wait_send()

        @pl.when(me > 0)
        def _():
            down.wait_send()

    for copy in gathers + pending:
        copy.wait_send()

    @pl.when(me > 0)
    def _():
        doc_prev.wait_send()

    @pl.when(me < n - 1)
    def _():
        doc_next.wait_send()


def solution(mesh):
    n, nt = mesh.shape["sp"], mesh.shape["tp"]
    try:
        xs = len({d.coords[0] for d in mesh.devices.flat})
    except AttributeError:
        xs = 2
    if n % xs or xs % 2:
        xs = 1

    def body(tokens, norm_gain, w_query, w_key, w_value, w_out, offset_bias, documents):
        layers, heads = offset_bias.shape[:2]
        toks, feat = tokens.shape
        model = nt * feat
        bias = jnp.pad(offset_bias, ((0, 0), (0, 0), (0, 0), (0, GRID_W - WIN_COLS)))
        bias = bias.reshape(layers * heads, WIN_ROWS * GRID_W)
        docs = documents.reshape(1, toks)
        reach = (WIN_ROWS // 2) * GRID_W
        dma = lambda *s: pltpu.SemaphoreType.DMA(s)
        vmem, hbm = pl.BlockSpec(memory_space=pltpu.VMEM), pl.BlockSpec(memory_space=pl.ANY)
        blocks = (layers, 2, toks, feat)
        return pl.pallas_call(
            functools.partial(kernel, n, nt, xs, layers, heads),
            out_shape=jax.ShapeDtypeStruct((toks, feat), BF16),
            in_specs=[vmem, vmem, hbm, hbm, hbm, hbm, vmem, vmem],
            out_specs=vmem,
            scratch_shapes=[
                pltpu.VMEM((layers, 3, model, feat), BF16),
                pltpu.VMEM((layers, n, feat, w_out.shape[2]), BF16),
                pltpu.VMEM((layers, nt, toks, feat), BF16),
                pltpu.VMEM((layers, 2 * reach - GRID_W + toks, 2 * feat), BF16),
                pltpu.VMEM(blocks, BF16),
                pltpu.VMEM(blocks, BF16),
                pltpu.VMEM(blocks, BF16),
                pltpu.VMEM(blocks, BF16),
                pltpu.VMEM((toks, feat), BF16),
                pltpu.VMEM((layers, heads, GRID_W, WIN_ROWS * GRID_W), F32),
                pltpu.VMEM((toks // GRID_W, GRID_W, WIN_ROWS * GRID_W), F32),
                pltpu.VMEM((3, 1, toks), jnp.int32),
                dma(layers, 4),
                dma(2, layers, n // 2, 4), dma(2, layers, n // 2, 4),
                dma(nt - 1), dma(nt - 1),
                dma(2, layers), dma(2, layers),
                dma(2), dma(2),
                dma(layers, 2), dma(layers, 2),
                dma(layers, 2), dma(layers, 2),
                dma(layers, 2), dma(layers, 2),
            ],
            compiler_params=pltpu.CompilerParams(
                collective_id=0, has_side_effects=True, vmem_limit_bytes=48 * 1024 * 1024
            ),
        )(tokens, norm_gain, w_query, w_key, w_value, w_out, bias, docs)

    return jax.shard_map(
        body,
        mesh=mesh,
        in_specs=(
            P("sp", "tp"),
            P(),
            P(None, "sp", "tp"),
            P(None, "sp", "tp"),
            P(None, "sp", "tp"),
            P(None, "tp", "sp"),
            P(None, "tp", None, None),
            P("sp"),
        ),
        out_specs=P("sp", "tp"),
        check_vma=False,
    )
```

time: 313 us -> 99.7 us (0.32)
  waiting for transfers between devices: 201 us -> 0 us
  Pallas kernels: 0 us -> 93.5 us
  starting transfers between devices: 25.1 us -> 0 us
  matrix products: 23 us -> 0 us
  blocking collectives: 20.8 us -> 0 us
  between operations: 14.2 us -> 0.02 us
  local copies, waits for them, and re-layouts: 19.3 us -> 5.89 us
  other arithmetic: 6.3 us -> 0 us
    all_gather x4 -> x0, waiting for transfers between devices: 144 us -> none  [the longest x1 43 us: body(): lax.all_gather(w_value, 'sp', axis=1, tiled=True)]
    pallas_call x0 -> x1, Pallas kernels: none -> 93.5 us  [body(): pl.pallas_call(functools.partial(kernel, n, nt, xs, layers, heads), out_s...]
    reduce_scatter x3 -> x0, waiting for transfers between devices: 48.7 us -> none  [body(): lax.psum_scatter(partial_sums.astype(jnp.bfloat16), 'tp', scatter_dimensi...]
    ppermute x8 -> x0, starting transfers between devices: 24.9 us -> none  [the longest x4 13.4 us: with_halo(): after = lax.ppermute(leading, axis, down)]
    dot_general x15 -> x0, matrix products: 21 us -> none  [the longest x3 5.98 us: body(): jnp.dot(attended, collected[3][layer_index], preferred_element_type=jnp.f...]
    all_gather x3 -> x0, blocking collectives: 20.8 us -> none  [body(): gathered = lax.all_gather(stream, 'tp', axis=1, tiled=True)]
    gather x6 -> x0, local copies, waits for them, and re-layouts: 14.4 us -> none  [attend(): bias_table = bias_layer[:, :, jnp.clip(col_offset, 0, WIN_COLS - 1)]]
    ppermute x8 -> x0, waiting for transfers between devices: 5.52 us -> none  [the longest x4 5.51 us: with_halo(): after = lax.ppermute(leading, axis, down)]
  transfers between devices with their start and end apart: 15 -> 0, of which waited for: 9 -> 0; matrix products, arithmetic and copies ran while one was open for 10% -> 0% of each run, Pallas kernels for 0% -> 0%
where the time goes in v1:
time: 99.7 us; the launch traced here: 99.4 us
  Pallas kernels  93.5 us (94%)
  local copies, waits for them, and re-layouts  5.89 us (6%)
    pallas_call x1, Pallas kernels, body(): pl.pallas_call(functools.partial(kernel, n, nt, xs, layers, heads), out_s...  93.5 us
    unnamed x15, local copies, waits for them, and re-layouts  4.97 us

profile of v1, /device:TPU:9, one launch (start us, length us, event | category | flops | bytes accessed | tf_op | source)
XLA Modules:
  0.0 99.4 jit_solution(8346743161510266931)
XLA Ops:
  0.0 0.0 copy-start.4
  0.0 0.8 pad.4
  0.8 0.0 copy-start.5
  0.8 0.0 copy-start.6
  0.8 0.1 reshape.6.bias_ref
  0.9 0.0 copy-done.4
  0.9 0.6 copy-done.5
  1.6 0.0 copy-done.6
  1.6 0.0 copy-start
  1.6 0.9 copy-done
  2.5 0.0 copy-start.1
  2.5 0.9 copy-done.1
  3.4 0.0 copy-start.2
  3.4 0.9 copy-done.2
  4.3 0.0 copy-start.3
  4.3 0.9 copy-done.3
  5.3 93.5 %shard_map.82 = bf16[128,256]{1,0:T(8,128)(2,1)S(1)} custom-call(bf16[128,256]{1,0:T(8,128)(2,1)S(1)} %copy-done.4, f32[3,1024]{1,0:T(4,128)S(1)} %copy-done.5, bf16[3,128,256]{2,1,0:T(8,128)(2,1)S(1)} %copy-done, bf16[3,128,256]{2,1,0:T(8,128)(2,1)S(1)} %copy-done.1, bf16[3,128,256]{2,1,0:T(8,128)(2,1)S(1)} %copy-done.2, ...), custom_call_target="tpu_custom_call" | custom-call | tf_op jit(solution)/shard_map/pallas_call | solution.py:356
  98.7 0.6 copy.10
Async XLA Ops:
  0.0 0.9 copy-start.4
  0.8 0.7 copy-start.5
  0.8 0.7 copy-start.6
  1.6 0.9 copy-start
  2.5 0.9 copy-start.1
  3.4 0.9 copy-start.2
  4.3 0.9 copy-start.3

commit v2 on v1

--- a/solution.py
+++ b/solution.py
@@ -70,7 +70,7 @@
 
     pl.semaphore_wait(barrier, 1 + nt + has_prev + has_next)
 
-    pending = []
+    pending, halos = [], []
 
     def remote(src, dst, send, recv, device):
         return pltpu.make_async_remote_copy(src_ref=src, dst_ref=dst, send_sem=send, recv_sem=recv,
@@ -104,8 +104,8 @@
         remote(ref, ref, w_send.at[direction, l, step - 1, c], w_recv.at[direction, l, step - 1, c],
                (right if direction == 0 else left, tp)).wait_recv()
 
-    def w_first(l):
-        for c in range(4):
+    def w_first(l, cs=range(4)):
+        for c in cs:
             owns[l * 4 + c].wait()
             for direction in range(2):
                 if c in w_chunks(direction, 1):
@@ -113,8 +113,8 @@
                     copy.start()
                     pending.append(copy)
 
-    def w_step(l, step):
-        for c in range(4):
+    def w_step(l, step, cs=range(4)):
+        for c in cs:
             for direction in range(2):
                 if c in w_chunks(direction, step):
                     w_arrive(direction, l, step, c)
@@ -125,10 +125,10 @@
 
     tasks = []
     for l in range(layers):
-        if l:
-            tasks.append((l, functools.partial(w_first, l)))
         for step in range(1, half + 1):
-            tasks.append((l, functools.partial(w_step, l, step)))
+            if step == half and l + 1 < layers:
+                tasks += [(l, functools.partial(w_first, l + 1, (c,))) for c in range(4)]
+            tasks += [(l, functools.partial(w_step, l, step, (c,))) for c in range(4)]
 
     def work(count, limit):
         while count > 0 and tasks and tasks[0][0] <= limit:
@@ -174,12 +174,7 @@
         for l in range(layers):
             kv[l, reach + toks:reach + toks + after] = jnp.zeros((after, 2 * feat), BF16)
 
-    for l in range(layers):
-        for h in range(heads):
-            row = jnp.broadcast_to(bias_ref[l * heads + h:l * heads + h + 1, :], (GRID_W, WIN_ROWS * GRID_W))
-            strip[l, h] = pltpu.roll(row, WIN_ROWS * GRID_W - WIN_COLS // 2, 1, stride=1, stride_axis=0)
-
-    work(1, 0)
+    work(4, 0)
 
     @pl.when(me > 0)
     def _():
@@ -197,12 +192,25 @@
     off = lane - col + WIN_COLS // 2
     inside = (off >= 0) & (off < WIN_COLS)
     rows = toks // GRID_W
+    wide = WIN_ROWS * GRID_W
     for r in range(rows):
         keys = seg_row[:, r * GRID_W:(r + WIN_ROWS) * GRID_W]
         mine = seg_col[r * GRID_W:(r + 1) * GRID_W, 0:1]
-        dmask[r] = jnp.where(inside & (keys == mine), 0.0, -1e30)
-
-    work(1, 0)
+        mask = jnp.where(inside & (keys == mine), 0.0, -1e30)
+        dmask[r * GRID_W:(r + 1) * GRID_W] = pltpu.roll(mask, r * GRID_W, 1) if r else mask
+
+    def fill_bias(l):
+        for h in range(heads):
+            row = jnp.broadcast_to(bias_ref[l * heads + h:l * heads + h + 1, :], (GRID_W, wide))
+            base = pltpu.roll(row, wide - WIN_COLS // 2, 1, stride=1, stride_axis=0)
+            for r in range(rows):
+                cut = slice(r * GRID_W, (r + 1) * GRID_W)
+                strip[l, h, cut] = (pltpu.roll(base, r * GRID_W, 1) if r else base) + dmask[cut]
+
+    fill_bias(0)
+    work(4, 0)
+    for l in range(1, layers):
+        fill_bias(l)
     for copy in gathers:
         copy.wait_recv()
 
@@ -224,47 +232,67 @@
             [(x[q] * inv * gain_ref[l:l + 1, q * feat:(q + 1) * feat]).astype(BF16) for q in range(nt)], axis=1)
         while tasks and tasks[0][0] <= l:
             work(1, l)
-        if l + 1 < layers:
-            work(1, l + 1)
 
         own = slice(reach, reach + toks)
-        kv[l, own, 0:feat] = head_norm(jnp.dot(normed, wbuf[l, K], preferred_element_type=F32), 1.0)
-        kv[l, own, feat:2 * feat] = jnp.dot(normed, wbuf[l, V], preferred_element_type=F32).astype(BF16)
-        up = to_next(kv.at[l, own], kv.at[l, 0:reach], l)
-        down = to_prev(kv.at[l, reach:reach + after], kv.at[l, reach + toks:reach + toks + after], l)
-
-        @pl.when(me < n - 1)
-        def _():
-            up.start()
-
-        @pl.when(me > 0)
-        def _():
-            down.start()
-
+        nxt = slice(reach + toks, reach + toks + after)
+        hops = []
+        for i, c in enumerate((K, V)):
+            lanes = slice(i * feat, (i + 1) * feat)
+            raw = jnp.dot(normed, wbuf[l, c], preferred_element_type=F32)
+            kv[l, own, lanes] = head_norm(raw, 1.0) if c == K else raw.astype(BF16)
+            up = to_next(kv.at[l, own, lanes], kv.at[l, 0:reach, lanes], 2 * l + i)
+            down = to_prev(kv.at[l, reach:reach + after, lanes], kv.at[l, nxt, lanes], 2 * l + i)
+            hops.append((up, down))
+
+            @pl.when(me < n - 1)
+            def _():
+                up.start()
+
+            @pl.when(me > 0)
+            def _():
+                down.start()
+
+        halos += hops
         query = head_norm(jnp.dot(normed, wbuf[l, Q], preferred_element_type=F32), HEAD_DIM ** -0.5)
-        work(1, l + 1)
-
-        @pl.when(me > 0)
-        def _():
-            up.wait_recv()
-
-        @pl.when(me < n - 1)
-        def _():
-            down.wait_recv()
-
+        work(4, l + 1)
+
+        part_o, part_d = [], []
         for h in range(heads):
             cut = slice(h * HEAD_DIM, (h + 1) * HEAD_DIM)
-            for r in range(rows):
-                win = slice(r * GRID_W, (r + WIN_ROWS) * GRID_W)
-                qr = query[r * GRID_W:(r + 1) * GRID_W, cut]
-                s = lax.dot_general(qr, kv[l, win, cut], (((1,), (1,)), ((), ())), preferred_element_type=F32)
-                p = jnp.exp(s + strip[l, h] + dmask[r])
-                den = jnp.sum(p, axis=-1, keepdims=True)
-                vals = kv[l, win, feat + h * HEAD_DIM:feat + (h + 1) * HEAD_DIM]
-                o = jnp.dot(p.astype(BF16), vals, preferred_element_type=F32)
-                att[r * GRID_W:(r + 1) * GRID_W, cut] = (o / den).astype(BF16)
-
-        work(1, l + 1)
+            s = lax.dot_general(query[:, cut], kv[l, own, cut], (((1,), (1,)), ((), ())),
+                                preferred_element_type=F32)
+            p = jnp.exp(s + strip[l, h, :, reach:])
+            part_d.append(jnp.sum(p, axis=-1, keepdims=True))
+            part_o.append(jnp.dot(p.astype(BF16), kv[l, own, feat + h * HEAD_DIM:feat + (h + 1) * HEAD_DIM],
+                                  preferred_element_type=F32))
+
+        for up, down in hops:
+            @pl.when(me > 0)
+            def _():
+                up.wait_recv()
+
+            @pl.when(me < n - 1)
+            def _():
+                down.wait_recv()
+
+        def halo(r, lanes):
+            seam = r * GRID_W
+            if not r:
+                return kv[l, 0:reach, lanes]
+            return jnp.concatenate([kv[l, reach + toks:reach + toks + seam, lanes], kv[l, seam:reach, lanes]], axis=0)
+
+        for r in range(rows):
+            keys, vals = halo(r, slice(0, feat)), halo(r, slice(feat, 2 * feat))
+            rcut = slice(r * GRID_W, (r + 1) * GRID_W)
+            for h in range(heads):
+                cut = slice(h * HEAD_DIM, (h + 1) * HEAD_DIM)
+                s = lax.dot_general(query[rcut, cut], keys[:, cut], (((1,), (1,)), ((), ())),
+                                    preferred_element_type=F32)
+                p = jnp.exp(s + strip[l, h, rcut, 0:reach])
+                den = jnp.sum(p, axis=-1, keepdims=True) + part_d[h][rcut]
+                o = jnp.dot(p.astype(BF16), vals[:, cut], preferred_element_type=F32) + part_o[h][rcut]
+                att[rcut, cut] = (o / den).astype(BF16)
+
         a = att[...]
         per = feat // wo_ref.shape[2]
 
@@ -280,6 +308,7 @@
             s1c.append(copy)
             pending.append(copy)
         mine = [mix(core + 2 * j) for j in range(2)]
+        work(4, l + 1)
         last = l == layers - 1
         if not last:
             s2c = []
@@ -290,7 +319,7 @@
                 copy.start()
                 s2c.append(copy)
                 pending.append(copy)
-            work(1, l + 1)
+            work(4, l + 1)
             s3c = []
             for j in range(2):
                 s2c[j].wait_recv()
@@ -313,6 +342,10 @@
             copy.wait_recv()
             out_ref[...] = (cs[l, y].astype(F32) + s2[l, 0].astype(F32)).astype(BF16)
 
+    for copy in gathers + pending:
+        copy.wait_send()
+
+    for up, down in halos:
         @pl.when(me < n - 1)
         def _():
             up.wait_send()
@@ -320,9 +353,6 @@
         @pl.when(me > 0)
         def _():
             down.wait_send()
-
-    for copy in gathers + pending:
-        copy.wait_send()
 
     @pl.when(me > 0)
     def _():
@@ -368,13 +398,13 @@
                 pltpu.VMEM(blocks, BF16),
                 pltpu.VMEM(blocks, BF16),
                 pltpu.VMEM((toks, feat), BF16),
-                pltpu.VMEM((layers, heads, GRID_W, WIN_ROWS * GRID_W), F32),
-                pltpu.VMEM((toks // GRID_W, GRID_W, WIN_ROWS * GRID_W), F32),
+                pltpu.VMEM((layers, heads, toks, WIN_ROWS * GRID_W), F32),
+                pltpu.VMEM((toks, WIN_ROWS * GRID_W), F32),
                 pltpu.VMEM((3, 1, toks), jnp.int32),
                 dma(layers, 4),
                 dma(2, layers, n // 2, 4), dma(2, layers, n // 2, 4),
                 dma(nt - 1), dma(nt - 1),
-                dma(2, layers), dma(2, layers),
+                dma(2, 2 * layers), dma(2, 2 * layers),
                 dma(2), dma(2),
                 dma(layers, 2), dma(layers, 2),
                 dma(layers, 2), dma(layers, 2),

time: 99.7 us -> 96.3 us (0.966); the launches traced: 99.4 us -> 94.8 us
  Pallas kernels: 93.5 us -> 88.9 us
    pallas_call x1, Pallas kernels: 93.5 us -> 88.9 us  [body(): pl.pallas_call(functools.partial(kernel, n, nt, xs, layers, heads), out_s...]
where the time goes in v2:
time: 96.3 us; the launch traced here: 94.8 us
  Pallas kernels  88.9 us (92%)
  local copies, waits for them, and re-layouts  5.89 us (6%)
    pallas_call x1, Pallas kernels, body(): pl.pallas_call(functools.partial(kernel, n, nt, xs, layers, heads), out_s...  88.9 us
    unnamed x15, local copies, waits for them, and re-layouts  4.97 us

profile of v2, /device:TPU:9, one launch (start us, length us, event | category | flops | bytes accessed | tf_op | source)
XLA Modules:
  0.0 94.8 jit_solution(15640570973276846650)
XLA Ops:
  0.0 0.0 copy-start.4
  0.0 0.8 pad.4
  0.8 0.0 copy-start.5
  0.8 0.0 copy-start.6
  0.8 0.1 reshape.6.bias_ref
  0.9 0.0 copy-done.4
  0.9 0.6 copy-done.5
  1.6 0.0 copy-done.6
  1.6 0.0 copy-start
  1.6 0.9 copy-done
  2.5 0.0 copy-start.1
  2.5 0.9 copy-done.1
  3.4 0.0 copy-start.2
  3.4 0.9 copy-done.2
  4.3 0.0 copy-start.3
  4.3 0.9 copy-done.3
  5.3 88.9 %shard_map.82 = bf16[128,256]{1,0:T(8,128)(2,1)S(1)} custom-call(bf16[128,256]{1,0:T(8,128)(2,1)S(1)} %copy-done.4, f32[3,1024]{1,0:T(4,128)S(1)} %copy-done.5, bf16[3,128,256]{2,1,0:T(8,128)(2,1)S(1)} %copy-done, bf16[3,128,256]{2,1,0:T(8,128)(2,1)S(1)} %copy-done.1, bf16[3,128,256]{2,1,0:T(8,128)(2,1)S(1)} %copy-done.2, ...), custom_call_target="tpu_custom_call" | custom-call | tf_op jit(solution)/shard_map/pallas_call | solution.py:386
  94.2 0.6 copy.10
Async XLA Ops:
  0.0 0.9 copy-start.4
  0.8 0.7 copy-start.5
  0.8 0.7 copy-start.6
  1.6 0.9 copy-start
  2.5 0.9 copy-start.1
  3.4 0.9 copy-start.2
  4.3 0.9 copy-start.3
